TPU v7x, 32 devices: a whole 2x2x4 slice. The times are simulated.
32 devices in a mesh: rep: 2 (over y), fs: 4 (over z), tp: 4 (over x, core).
Axes of the slice: x: 2, y: 2, z: 4, core: 2. Of those that a mesh axis runs over, the one named last changes fastest.
Arguments:
- out_grad: bfloat16 [2048, 2048], P(('rep', 'fs'), 'tp'), may hold values from -6 to 6
- gate_lin: bfloat16 [2048, 5632], P(('rep', 'fs'), 'tp'), may hold values from -6 to 6
- up_lin: bfloat16 [2048, 5632], P(('rep', 'fs'), 'tp'), may hold values from -6 to 6
- conv_weight: bfloat16 [3, 5632], replicated, may hold values from -3.5 to 3.5
- gate_weight: bfloat16 [2048, 5632], P('fs', 'tp'), may hold values from -0.125 to 0.125
- up_weight: bfloat16 [2048, 5632], P('fs', 'tp'), may hold values from -0.125 to 0.125
- down_weight: bfloat16 [5632, 2048], P('tp', 'fs'), may hold values from -0.078125 to 0.078125
Outputs:
- input_grad: bfloat16 [2048, 2048], P(('rep', 'fs'), 'tp')
- conv_grad: float32 [3, 5632], replicated
All inputs are finite; a program needn't handle non-finite values.
Results may differ from a plain program's by a relative error of at most 0.015.
Values may be sent and summed in bfloat16 or wider, within the bound.
A program may use at most 64 MiB of HBM per device.

v0:
```python
import math
import jax
import jax.numpy as jnp
from jax import lax
from jax.sharding import PartitionSpec as P


def extended(value, sides, width):
    for axis, dim in sides:
        peers, length = (lax.axis_size(axis), value.shape[dim])
        up = [(i, (i + 1) % peers) for i in range(peers - 1)]
        down = [(j, i) for i, j in up]
        last = lax.slice_in_dim(value, length - width, length, axis=dim)
        leading = lax.slice_in_dim(value, 0, width, axis=dim)
        before = lax.ppermute(last, axis, up)
        after = lax.ppermute(leading, axis, down)
        value = jnp.concatenate([before, value, after], axis=dim)
    return value


def gelu_parts(gate):
    normal_cdf = 0.5 * (1.0 + jax.scipy.special.erf(gate * (1.0 / math.sqrt(2.0))))
    density = jnp.exp(-0.5 * gate * gate) * (1.0 / math.sqrt(2.0 * math.pi))
    return (gate * normal_cdf, normal_cdf + gate * density)


def local(out_grad, gate_lin, up_lin, conv_weight, gate_weight, up_weight, down_weight):
    conv_full = conv_weight.astype(jnp.float32)
    column_count = gate_lin.shape[1]
    column_start = lax.axis_index("tp") * column_count
    conv_taps = lax.dynamic_slice_in_dim(conv_full, column_start, column_count, 1)
    grad_rows = lax.all_gather(out_grad, "tp", axis=1, tiled=True)
    act_grad = lax.dot_general(
        grad_rows,
        lax.all_gather(down_weight, "fs", axis=1, tiled=True),
        (((1,), (1,)), ((), ())),
        preferred_element_type=jnp.float32,
    )
    linear_mid = extended(gate_lin, (("fs", 0),), 1).astype(jnp.float32)
    gate = (
        conv_taps[0] * linear_mid[:-2]
        + conv_taps[1] * linear_mid[1:-1]
        + conv_taps[2] * linear_mid[2:]
    )
    gelu_value, gelu_slope = gelu_parts(gate)
    gate_grad = act_grad * up_lin.astype(jnp.float32) * gelu_slope
    grad_ext = extended(gate_grad.astype(jnp.bfloat16), (("fs", 0),), 1).astype(gate_grad.dtype)
    up_grad = (act_grad * gelu_value).astype(jnp.bfloat16)
    own_grad = grad_ext[1:-1]
    linear_grad = (
        conv_taps[0] * grad_ext[2:] + conv_taps[1] * own_grad + conv_taps[2] * grad_ext[:-2]
    ).astype(jnp.bfloat16)
    local_conv = jnp.stack(
        [
            jnp.sum(own_grad * linear_mid[:-2], axis=0),
            jnp.sum(own_grad * linear_mid[1:-1], axis=0),
            jnp.sum(own_grad * linear_mid[2:], axis=0),
        ]
    )
    product = lax.dot_general(
        linear_grad,
        lax.all_gather(gate_weight, "fs", axis=0, tiled=True),
        (((1,), (1,)), ((), ())),
        preferred_element_type=jnp.float32,
    )
    product = product + lax.dot_general(
        up_grad,
        lax.all_gather(up_weight, "fs", axis=0, tiled=True),
        (((1,), (1,)), ((), ())),
        preferred_element_type=jnp.float32,
    )
    input_grad = lax.psum_scatter(
        product.astype(jnp.bfloat16), "tp", scatter_dimension=1, tiled=True
    )
    summed_conv = lax.psum(local_conv, ("rep", "fs"))
    conv_grad = lax.all_gather(summed_conv, "tp", axis=1, tiled=True)
    return (input_grad, conv_grad)


def solution(mesh):
    return jax.shard_map(
        local,
        mesh=mesh,
        in_specs=(
            P(("rep", "fs"), "tp"),
            P(("rep", "fs"), "tp"),
            P(("rep", "fs"), "tp"),
            P(),
            P("fs", "tp"),
            P("fs", "tp"),
            P("tp", "fs"),
        ),
        out_specs=(P(("rep", "fs"), "tp"), P()),
        check_vma=False,
    )
```

profile of v0, /device:TPU:0, one launch (start us, length us, event | category | flops | bytes accessed | tf_op | source)
XLA Modules:
  0.0 404.9 jit_solution(1864692760127615159)
XLA Ops:
  7.2 0.7 all-gather.5.cloned.1.call-update
  7.9 0.7 all-gather.7.cloned.1.call-update
  8.7 0.7 all-gather.9.cloned.1.call-update
  9.4 0.5 all-gather.11.cloned.1.call-update
  10.1 5.1 %collective-permute-start = (bf16[1,1408]{1,0:T(2,128)(2,1)S(1)}, bf16[1,1408]{1,0:T(2,128)(2,1)S(1)}, u32[]{:S(2)}, u32[]{:S(2)}) collective-permute-start(bf16[1,1408]{1,0:T(2,128)(2,1)S(1)} %get-tuple-element.12), channel_id=1, source_target_pairs={{0,4},{4,8},{8,12},{1,5},{5,9},{9,13},{2,6},{6,10},{10,14},{3,7},{... | collective-permute-start | bytes 8456 | tf_op jit(solution)/shard_map/ppermute | solution.py:15
  15.2 1.3 collective-permute-start.1
  16.5 0.7 dynamic-slice_convert_fusion
  17.2 3.4 collective-permute-done.1
  20.7 0.2 maximum_convert_fusion
  20.8 8.2 %all-gather.5.cloned.1.call-done = bf16[256,2048]{1,0:T(8,128)(2,1)} async-done(((bf16[256,512]{1,0:T(8,128)(2,1)}), bf16[256,2048]{1,0:T(8,128)(2,1)}) %all-gather.5.cloned.1.call-update) | async-done | bytes 1048592 | tf_op jit(solution)/shard_map/all_gather | solution.py:32
  29.0 108.3 %all-gather.7.cloned.1.call-done = bf16[1408,2048]{1,0:T(8,128)(2,1)} async-done(((bf16[1408,512]{1,0:T(8,128)(2,1)}), bf16[1408,2048]{1,0:T(8,128)(2,1)}) %all-gather.7.cloned.1.call-update) | async-done | bytes 5767184 | tf_op jit(solution)/shard_map/all_gather | solution.py:35
  137.3 7.2 %fusion.6 = (bf16[256,1408]{1,0:T(8,128)(2,1)S(1)}, f32[256,1408]{1,0:T(8,128)}, f32[256,1408]{1,0:T(8,128)}) fusion(bf16[256,1408]{1,0:T(8,128)(2,1)S(1)} %copy-done.1, f32[258,1408]{1,0:T(8,128)S(1)} %maximum_convert_fusion, f32[1408]{0:T(1024)S(1)} %get-tuple-element.7, f32[1408]{0:T(1024)S(1)} %get-tuple-element.6, f32[1408]{0:T(1024)S(1)} %get-tuple-element.5, ...), kind=kOutput, calls=%fused_computation.8 | convolution fusion | flops 1482522624 | bytes 15483392 | tf_op jit(solution)/shard_map/dot_general | solution.py:33
  144.5 1.3 collective-permute-start.2
  145.8 1.3 collective-permute-start.3
  147.1 4.4 %collective-permute-done.3 = bf16[1,1408]{1,0:T(2,128)(2,1)S(1)} collective-permute-done((bf16[1,1408]{1,0:T(2,128)(2,1)S(1)}, bf16[1,1408]{1,0:T(2,128)(2,1)S(1)}, u32[]{:S(2)}, u32[]{:S(2)}) %collective-permute-start.3) | collective-permute-done | bytes 2848 | tf_op jit(solution)/shard_map/ppermute | solution.py:16
  151.5 0.2 maximum_convert_fusion.1
  151.7 92.3 %all-gather.9.cloned.1.call-done = bf16[2048,1408]{1,0:T(8,128)(2,1)} async-done(((bf16[512,1408]{1,0:T(8,128)(2,1)}), bf16[2048,1408]{1,0:T(8,128)(2,1)}) %all-gather.9.cloned.1.call-update) | async-done | bytes 5767184 | tf_op jit(solution)/shard_map/all_gather | solution.py:62
  244.0 6.0 %fusion.10 = f32[256,2048]{1,0:T(8,128)} fusion(bf16[2048,1408]{1,0:T(8,128)(2,1)} %all-gather.9.cloned.1.call-done, f32[258,1408]{1,0:T(8,128)S(1)} %maximum_convert_fusion.1, f32[1408]{0:T(1024)S(1)} %get-tuple-element.7, f32[1408]{0:T(1024)S(1)} %get-tuple-element.6, f32[1408]{0:T(1024)S(1)} %get-tuple-element.5), kind=kOutput, calls=%fused_computation.22 | convolution fusion | flops 1478557696 | bytes 12214272 | tf_op jit(solution)/shard_map/dot_general | solution.py:60
  249.9 100.4 %all-gather.11.cloned.1.call-done = bf16[2048,1408]{1,0:T(8,128)(2,1)} async-done(((bf16[512,1408]{1,0:T(8,128)(2,1)}), bf16[2048,1408]{1,0:T(8,128)(2,1)}) %all-gather.11.cloned.1.call-update) | async-done | bytes 5767184 | tf_op jit(solution)/shard_map/all_gather | solution.py:68
  350.3 6.9 %fusion = bf16[256,2048]{1,0:T(8,128)(2,1)} fusion(f32[256,2048]{1,0:T(8,128)} %fusion.10, bf16[2048,1408]{1,0:T(8,128)(2,1)} %all-gather.11.cloned.1.call-done, f32[256,1408]{1,0:T(8,128)} %get-tuple-element.14, f32[256,1408]{1,0:T(8,128)} %get-tuple-element.9), kind=kOutput, calls=%fused_computation.1 | convolution fusion | flops 1479606272 | bytes 11796480 | tf_op jit(solution)/shard_map/dot_general | solution.py:66
  357.3 0.6 multiply_reduce_fusion.2
  357.9 34.5 %psum.7 = f32[3,1408]{1,0:T(4,128)S(1)} all-reduce(f32[3,1408]{1,0:T(4,128)S(1)} %pad_maximum_fusion), channel_id=1, replica_groups=mesh['rep'=2,'fs'=4,'tp'=4] {'rep','fs'}, use_global_device_ids=true, to_apply=%region_4.0 | all-reduce | flops 4224 | bytes 33792 | tf_op jit(solution)/shard_map/psum | solution.py:75
  392.4 5.3 %all_gather.19 = f32[3,5632]{1,0:T(4,128)S(1)} all-gather(f32[3,1408]{1,0:T(4,128)S(1)} %psum.7), channel_id=1, replica_groups=mesh['rep'=2,'fs'=4,'tp'=4] {'tp'}, dimensions={1}, use_global_device_ids=true | all-gather | bytes 84480 | tf_op jit(solution)/shard_map/all_gather | solution.py:76
  397.7 0.6 copy.10
  (20 shorter events, 0.4 us)
Async XLA Ops:
  7.2 21.8 %all-gather.5.cloned.1.call-start = ((), (), s32[]{:S(2)}) async-start(), calls=%async_computation.1 | async-start | bytes 1310720 | tf_op jit(solution)/shard_map/all_gather | solution.py:32
  7.9 129.4 %all-gather.7.cloned.1.call-start = ((), (), s32[]{:S(2)}) async-start(), calls=%async_computation.2 | async-start | bytes 7208960 | tf_op jit(solution)/shard_map/all_gather | solution.py:35
  8.6 1.4 copy-start
  8.7 235.3 %all-gather.9.cloned.1.call-start = ((), (), s32[]{:S(2)}) async-start(), calls=%async_computation.3 | async-start | bytes 7208960 | tf_op jit(solution)/shard_map/all_gather | solution.py:62
  9.4 340.9 %all-gather.11.cloned.1.call-start = ((), (), s32[]{:S(2)}) async-start(), calls=%async_computation.4 | async-start | bytes 7208960 | tf_op jit(solution)/shard_map/all_gather | solution.py:68
  10.0 127.3 %copy-start.1 = (bf16[256,1408]{1,0:T(8,128)(2,1)S(1)}, bf16[256,1408]{1,0:T(8,128)(2,1)}, u32[]{:S(2)}) copy-start(bf16[256,1408]{1,0:T(8,128)(2,1)} %param.9) | copy-start | bytes 2162692
  10.0 387.7 %reduce-scatter.2.cloned.1.call-start = ((), (), s32[]{:S(2)}) async-start(), calls=%async_computation.5 | async-start | bytes 1310720 | tf_op jit(solution)/shard_map/reduce_scatter | solution.py:72
  10.1 7.2 %collective-permute-start = (bf16[1,1408]{1,0:T(2,128)(2,1)S(1)}, bf16[1,1408]{1,0:T(2,128)(2,1)S(1)}, u32[]{:S(2)}, u32[]{:S(2)}) collective-permute-start(bf16[1,1408]{1,0:T(2,128)(2,1)S(1)} %get-tuple-element.12), channel_id=1, source_target_pairs={{0,4},{4,8},{8,12},{1,5},{5,9},{9,13},{2,6},{6,10},{10,14},{3,7},{... | collective-permute-start | bytes 8456 | tf_op jit(solution)/shard_map/ppermute | solution.py:15
  15.2 5.5 %collective-permute-start.1 = (bf16[1,1408]{1,0:T(2,128)(2,1)S(1)}, bf16[1,1408]{1,0:T(2,128)(2,1)S(1)}, u32[]{:S(2)}, u32[]{:S(2)}) collective-permute-start(bf16[1,1408]{1,0:T(2,128)(2,1)S(1)} %get-tuple-element.13), channel_id=1, source_target_pairs={{4,0},{8,4},{12,8},{5,1},{9,5},{13,9},{6,2},{10,6},{14,10},{7,3},{... | collective-permute-start | bytes 8456 | tf_op jit(solution)/shard_map/ppermute | solution.py:16
  144.5 2.6 collective-permute-start.2
  145.8 5.8 %collective-permute-start.3 = (bf16[1,1408]{1,0:T(2,128)(2,1)S(1)}, bf16[1,1408]{1,0:T(2,128)(2,1)S(1)}, u32[]{:S(2)}, u32[]{:S(2)}) collective-permute-start(bf16[1,1408]{1,0:T(2,128)(2,1)S(1)} %get-tuple-element.11), channel_id=1, source_target_pairs={{4,0},{8,4},{12,8},{5,1},{9,5},{13,9},{6,2},{10,6},{14,10},{7,3},{... | collective-permute-start | bytes 8456 | tf_op jit(solution)/shard_map/ppermute | solution.py:16
Sparse Core Ops, SparseCore 0:
  9.5 19.4 all-gather.4
  30.6 106.6 all-gather.6
  138.9 105.0 all-gather.8
  245.4 104.8 all-gather.10
  357.4 23.0 reduce-scatter.1
where the time goes:
time: 405 us
  waiting for transfers between devices  320 us (79%)
  blocking collectives  39.8 us (10%)
  matrix products  20.1 us (5%)
  between operations  13.9 us (3%)
  starting transfers between devices  9.15 us (2%)
    all_gather x1, waiting for transfers between devices, local(): lax.all_gather(down_weight, 'fs', axis=1, tiled=True)  108 us
    all_gather x1, waiting for transfers between devices, local(): lax.all_gather(up_weight, 'fs', axis=0, tiled=True)  100 us
    all_gather x1, waiting for transfers between devices, local(): lax.all_gather(gate_weight, 'fs', axis=0, tiled=True)  92.3 us
    psum x1, blocking collectives, local(): summed_conv = lax.psum(local_conv, ('rep', 'fs'))  34.5 us
    all_gather x1, waiting for transfers between devices, local(): grad_rows = lax.all_gather(out_grad, 'tp', axis=1, tiled=True)  8.16 us
  transfers between devices with their start and end apart: 9, of which 6 were waited for; matrix products, arithmetic and copies ran while one was open for 4% of the time, Pallas kernels for 0%

commit v1 on v0

--- a/solution.py
+++ b/solution.py
@@ -3,6 +3,23 @@
 import jax.numpy as jnp
 from jax import lax
 from jax.sharding import PartitionSpec as P
+
+
+def in_order(pieces, dim):
+    lengths = list(pieces.shape[1:])
+    lengths[dim] *= pieces.shape[0]
+    return jnp.moveaxis(pieces, 0, dim).reshape(lengths)
+
+
+def ring_gather(x, axis, dim):
+    size = lax.axis_size(axis)
+    forward = [(i, (i + 1) % size) for i in range(size)]
+    tiles = [x]
+    while len(tiles) < size:
+        tiles.append(lax.ppermute(tiles[-1], axis, forward))
+    index = lax.axis_index(axis)
+    tiles = jnp.stack(tiles)[(index - jnp.arange(size)) % size]
+    return in_order(tiles, dim)
 
 
 def extended(value, sides, width):
@@ -32,7 +49,7 @@
     grad_rows = lax.all_gather(out_grad, "tp", axis=1, tiled=True)
     act_grad = lax.dot_general(
         grad_rows,
-        lax.all_gather(down_weight, "fs", axis=1, tiled=True),
+        ring_gather(down_weight, "fs", 1),
         (((1,), (1,)), ((), ())),
         preferred_element_type=jnp.float32,
     )

time: 405 us -> 363 us (0.90)
  waiting for transfers between devices: 320 us -> 215 us
  starting transfers between devices: 9.15 us -> 48.5 us
  local copies, waits for them, and re-layouts: 0.74 us -> 17.5 us
  other arithmetic: 1.66 us -> 7.76 us
    all_gather x1 -> x0, waiting for transfers between devices: 108 us -> none  [local(): lax.all_gather(down_weight, 'fs', axis=1, tiled=True)]
    ppermute x0 -> x3, waiting for transfers between devices: none -> 104 us  [ring_gather(): tiles.append(lax.ppermute(tiles[-1], axis, forward))]
    all_gather x1, waiting for transfers between devices: 92.3 us -> 0.02 us  [local(): lax.all_gather(gate_weight, 'fs', axis=0, tiled=True)]
    ppermute x2, waiting for transfers between devices: 0.03 us -> 39.3 us  [extended(): before = lax.ppermute(last, axis, up)]
    ppermute x0 -> x3, starting transfers between devices: none -> 38.1 us  [ring_gather(): tiles.append(lax.ppermute(tiles[-1], axis, forward))]
    all_gather x1, waiting for transfers between devices: 100 us -> 63.7 us  [local(): lax.all_gather(up_weight, 'fs', axis=0, tiled=True)]
    transpose x0 -> x1, local copies, waits for them, and re-layouts: none -> 8.42 us  [in_order(): return jnp.moveaxis(pieces, 0, dim).reshape(lengths)]
    all_gather x1, waiting for transfers between devices: 8.16 us -> 0.01 us  [local(): grad_rows = lax.all_gather(out_grad, 'tp', axis=1, tiled=True)]
  transfers between devices with their start and end apart: 9 -> 11, of which waited for: 6 -> 7; matrix products, arithmetic and copies ran while one was open for 4% -> 10% of each run, Pallas kernels for 0% -> 0%
where the time goes in v1:
time: 363 us
  waiting for transfers between devices  215 us (59%)
  starting transfers between devices  48.5 us (13%)
  blocking collectives  39.8 us (11%)
  matrix products  19.9 us (5%)
  local copies, waits for them, and re-layouts  17.5 us (5%)
  between operations  13.9 us (4%)
  other arithmetic  7.76 us (2%)
    ppermute x3, waiting for transfers between devices, ring_gather(): tiles.append(lax.ppermute(tiles[-1], axis, forward))  104 us
    all_gather x1, waiting for transfers between devices, local(): lax.all_gather(up_weight, 'fs', axis=0, tiled=True)  63.7 us
    ppermute x2, waiting for transfers between devices, extended(): before = lax.ppermute(last, axis, up)  39.3 us
    ppermute x3, starting transfers between devices, ring_gather(): tiles.append(lax.ppermute(tiles[-1], axis, forward))  38.1 us
    psum x1, blocking collectives, local(): summed_conv = lax.psum(local_conv, ('rep', 'fs'))  34.5 us
    transpose x1, local copies, waits for them, and re-layouts, in_order(): return jnp.moveaxis(pieces, 0, dim).reshape(lengths)  8.42 us
    ppermute x2, starting transfers between devices, extended(): before = lax.ppermute(last, axis, up)  7.6 us
  transfers between devices with their start and end apart: 11, of which 7 were waited for; matrix products, arithmetic and copies ran while one was open for 10% of the time, Pallas kernels for 0%

profile of v1, /device:TPU:0, one launch (start us, length us, event | category | flops | bytes accessed | tf_op | source)
XLA Modules:
  0.0 362.5 jit_solution(1436198434852577471)
XLA Ops:
  9.4 3.1 collective-permute-start
  12.6 36.9 %collective-permute-done = bf16[1408,512]{1,0:T(8,128)(2,1)S(1)} collective-permute-done((bf16[1408,512]{1,0:T(8,128)(2,1)S(1)}, bf16[1408,512]{1,0:T(8,128)(2,1)S(1)}, u32[]{:S(2)}, u32[]{:S(2)}) %collective-permute-start) | collective-permute-done | bytes 1441824 | tf_op jit(solution)/shard_map/ppermute | solution.py:19
  49.4 1.1 copy-done.1
  50.6 3.4 collective-permute-start.1
  53.9 65.4 %collective-permute-done.1 = bf16[1408,512]{1,0:T(8,128)(2,1)} collective-permute-done((bf16[1408,512]{1,0:T(8,128)(2,1)S(1)}, bf16[1408,512]{1,0:T(8,128)(2,1)}, u32[]{:S(2)}, u32[]{:S(2)}) %collective-permute-start.1) | collective-permute-done | bytes 1441824 | tf_op jit(solution)/shard_map/ppermute | solution.py:19
  119.3 31.7 %collective-permute-start.2 = (bf16[1408,512]{1,0:T(8,128)(2,1)}, bf16[1408,512]{1,0:T(8,128)(2,1)}, u32[]{:S(2)}, u32[]{:S(2)}) collective-permute-start(bf16[1408,512]{1,0:T(8,128)(2,1)} %collective-permute-done.1), channel_id=1, source_target_pairs={{0,4},{4,8},{8,12},{12,0},{1,5},{5,9},{9,13},{13,1},{2,6},{6,10},{... | collective-permute-start | bytes 4325384 | tf_op jit(solution)/shard_map/ppermute | solution.py:19
  151.7 5.0 %collective-permute-start.3 = (bf16[1,1408]{1,0:T(2,128)(2,1)S(1)}, bf16[1,1408]{1,0:T(2,128)(2,1)S(1)}, u32[]{:S(2)}, u32[]{:S(2)}) collective-permute-start(bf16[1,1408]{1,0:T(2,128)(2,1)S(1)} %get-tuple-element.12), channel_id=1, source_target_pairs={{0,4},{4,8},{8,12},{1,5},{5,9},{9,13},{2,6},{6,10},{10,14},{3,7},{... | collective-permute-start | bytes 8456 | tf_op jit(solution)/shard_map/ppermute | solution.py:32
  156.7 1.3 collective-permute-start.4
  158.1 0.8 dynamic-slice_convert_fusion
  159.0 39.3 %collective-permute-done.3 = bf16[1,1408]{1,0:T(2,128)(2,1)S(1)} collective-permute-done((bf16[1,1408]{1,0:T(2,128)(2,1)S(1)}, bf16[1,1408]{1,0:T(2,128)(2,1)S(1)}, u32[]{:S(2)}, u32[]{:S(2)}) %collective-permute-start.3) | collective-permute-done | bytes 2848 | tf_op jit(solution)/shard_map/ppermute | solution.py:32
  198.2 1.3 maximum_convert_fusion
  199.5 1.6 collective-permute-done.2
  201.1 4.9 %pad_maximum_fusion = bf16[4,1408,512]{2,1,0:T(8,128)(2,1)} fusion(bf16[1,1408,512]{2,1,0:T(8,128)(2,1)} %bitcast.3, bf16[1,1408,512]{2,1,0:T(8,128)(2,1)} %bitcast.2, bf16[1,1408,512]{2,1,0:T(8,128)(2,1)S(1)} %bitcast.17, bf16[1,1408,512]{2,1,0:T(8,128)(2,1)S(1)} %bitcast.16), kind=kLoop, calls=%fused_computation.1 | loop fusion | flops 8650752 | bytes 11534336 | tf_op jit(solution)/shard_map/stack | solution.py:21
  205.9 6.4 %gather_fusion = bf16[4,1408,512]{2,1,0:T(8,128)(2,1)} fusion(bf16[4,1408,512]{2,1,0:T(8,128)(2,1)} %pad_maximum_fusion, s32[1024]{0:T(1024)S(1)} %pad_clamp_fusion), kind=kCustom, calls=%fused_computation | custom fusion | bytes 11534352 | tf_op jit(solution)/shard_map/gather | solution.py:21
  212.4 8.4 %copy.9 = bf16[1408,4,512]{0,2,1:T(8,128)(2,1)} copy(bf16[1408,4,512]{2,0,1:T(8,128)(2,1)} %bitcast.14) | data formatting | bytes 11534336 | tf_op jit(solution)/shard_map/transpose | solution.py:11
  220.8 7.0 %fusion.6 = (bf16[256,1408]{1,0:T(8,128)(2,1)S(1)}, f32[256,1408]{1,0:T(8,128)}, f32[256,1408]{1,0:T(8,128)}) fusion(bf16[256,1408]{1,0:T(8,128)(2,1)S(1)} %copy-done.3, f32[258,1408]{1,0:T(8,128)S(1)} %maximum_convert_fusion, f32[1408]{0:T(1024)S(1)} %get-tuple-element.7, f32[1408]{0:T(1024)S(1)} %get-tuple-element.6, f32[1408]{0:T(1024)S(1)} %get-tuple-element.5, ...), kind=kOutput, calls=%fused_computation.11 | convolution fusion | flops 1482522624 | bytes 15483392 | tf_op jit(solution)/shard_map/dot_general | solution.py:50
  227.8 2.6 collective-permute-start.5
  230.4 1.3 collective-permute-start.6
  231.8 6.2 %collective-permute-done.6 = bf16[1,1408]{1,0:T(2,128)(2,1)S(1)} collective-permute-done((bf16[1,1408]{1,0:T(2,128)(2,1)S(1)}, bf16[1,1408]{1,0:T(2,128)(2,1)S(1)}, u32[]{:S(2)}, u32[]{:S(2)}) %collective-permute-start.6) | collective-permute-done | bytes 2848 | tf_op jit(solution)/shard_map/ppermute | solution.py:33
  238.2 6.0 %fusion.10 = f32[256,2048]{1,0:T(8,128)} fusion(bf16[2048,1408]{1,0:T(8,128)(2,1)} %all-gather.6.cloned.1.call-done, f32[258,1408]{1,0:T(8,128)S(1)} %maximum_convert_fusion.1, f32[1408]{0:T(1024)S(1)} %get-tuple-element.7, f32[1408]{0:T(1024)S(1)} %get-tuple-element.6, f32[1408]{0:T(1024)S(1)} %get-tuple-element.5), kind=kOutput, calls=%fused_computation.25 | convolution fusion | flops 1478557696 | bytes 12214272 | tf_op jit(solution)/shard_map/dot_general | solution.py:77
  244.2 63.7 %all-gather.8.cloned.1.call-done = bf16[2048,1408]{1,0:T(8,128)(2,1)} async-done(((bf16[512,1408]{1,0:T(8,128)(2,1)}), bf16[2048,1408]{1,0:T(8,128)(2,1)}) %all-gather.8.cloned.1.call-update) | async-done | bytes 5767184 | tf_op jit(solution)/shard_map/all_gather | solution.py:85
  307.9 6.9 %fusion = bf16[256,2048]{1,0:T(8,128)(2,1)} fusion(f32[256,2048]{1,0:T(8,128)} %fusion.10, bf16[2048,1408]{1,0:T(8,128)(2,1)} %all-gather.8.cloned.1.call-done, f32[256,1408]{1,0:T(8,128)} %get-tuple-element.14, f32[256,1408]{1,0:T(8,128)} %get-tuple-element.9), kind=kOutput, calls=%fused_computation.4 | convolution fusion | flops 1479606272 | bytes 11796480 | tf_op jit(solution)/shard_map/dot_general | solution.py:83
  315.5 34.5 %psum.7 = f32[3,1408]{1,0:T(4,128)S(1)} all-reduce(f32[3,1408]{1,0:T(4,128)S(1)} %pad_maximum_fusion.1), channel_id=1, replica_groups=mesh['rep'=2,'fs'=4,'tp'=4] {'rep','fs'}, use_global_device_ids=true, to_apply=%region_4.5 | all-reduce | flops 4224 | bytes 33792 | tf_op jit(solution)/shard_map/psum | solution.py:92
  350.1 5.3 %all_gather.15 = f32[3,5632]{1,0:T(4,128)S(1)} all-gather(f32[3,1408]{1,0:T(4,128)S(1)} %psum.7), channel_id=1, replica_groups=mesh['rep'=2,'fs'=4,'tp'=4] {'tp'}, dimensions={1}, use_global_device_ids=true | all-gather | bytes 84480 | tf_op jit(solution)/shard_map/all_gather | solution.py:93
  (32 shorter events, 4.6 us)
Async XLA Ops:
  7.2 213.6 %all-gather.4.cloned.1.call-start = ((), (), s32[]{:S(2)}) async-start(), calls=%async_computation.1 | async-start | bytes 1310720 | tf_op jit(solution)/shard_map/all_gather | solution.py:49
  7.9 1.5 copy-start
  7.9 230.3 %all-gather.6.cloned.1.call-start = ((), (), s32[]{:S(2)}) async-start(), calls=%async_computation.2 | async-start | bytes 7208960 | tf_op jit(solution)/shard_map/all_gather | solution.py:79
  8.7 299.3 %all-gather.8.cloned.1.call-start = ((), (), s32[]{:S(2)}) async-start(), calls=%async_computation.3 | async-start | bytes 7208960 | tf_op jit(solution)/shard_map/all_gather | solution.py:85
  9.4 346.0 %reduce-scatter.2.cloned.1.call-start = ((), (), s32[]{:S(2)}) async-start(), calls=%async_computation.4 | async-start | bytes 1310720 | tf_op jit(solution)/shard_map/reduce_scatter | solution.py:89
  9.4 40.0 %collective-permute-start = (bf16[1408,512]{1,0:T(8,128)(2,1)S(1)}, bf16[1408,512]{1,0:T(8,128)(2,1)S(1)}, u32[]{:S(2)}, u32[]{:S(2)}) collective-permute-start(bf16[1408,512]{1,0:T(8,128)(2,1)S(1)} %copy-done), channel_id=1, source_target_pairs={{0,4},{4,8},{8,12},{12,0},{1,5},{5,9},{9,13},{13,1},{2,6},{6,10},{... | collective-permute-start | bytes 4325384 | tf_op jit(solution)/shard_map/ppermute | solution.py:19
  49.4 1.1 copy-start.1
  50.6 68.7 %collective-permute-start.1 = (bf16[1408,512]{1,0:T(8,128)(2,1)S(1)}, bf16[1408,512]{1,0:T(8,128)(2,1)}, u32[]{:S(2)}, u32[]{:S(2)}) collective-permute-start(bf16[1408,512]{1,0:T(8,128)(2,1)S(1)} %collective-permute-done), channel_id=1, source_target_pairs={{0,4},{4,8},{8,12},{12,0},{1,5},{5,9},{9,13},{13,1},{2,6},{6,10},{... | collective-permute-start | bytes 4325384 | tf_op jit(solution)/shard_map/ppermute | solution.py:19
  119.3 81.8 %collective-permute-start.2 = (bf16[1408,512]{1,0:T(8,128)(2,1)}, bf16[1408,512]{1,0:T(8,128)(2,1)}, u32[]{:S(2)}, u32[]{:S(2)}) collective-permute-start(bf16[1408,512]{1,0:T(8,128)(2,1)} %collective-permute-done.1), channel_id=1, source_target_pairs={{0,4},{4,8},{8,12},{12,0},{1,5},{5,9},{9,13},{13,1},{2,6},{6,10},{... | collective-permute-start | bytes 4325384 | tf_op jit(solution)/shard_map/ppermute | solution.py:19
  151.7 46.5 %collective-permute-start.3 = (bf16[1,1408]{1,0:T(2,128)(2,1)S(1)}, bf16[1,1408]{1,0:T(2,128)(2,1)S(1)}, u32[]{:S(2)}, u32[]{:S(2)}) collective-permute-start(bf16[1,1408]{1,0:T(2,128)(2,1)S(1)} %get-tuple-element.12), channel_id=1, source_target_pairs={{0,4},{4,8},{8,12},{1,5},{5,9},{9,13},{2,6},{6,10},{10,14},{3,7},{... | collective-permute-start | bytes 8456 | tf_op jit(solution)/shard_map/ppermute | solution.py:32
  156.7 41.5 %collective-permute-start.4 = (bf16[1,1408]{1,0:T(2,128)(2,1)S(1)}, bf16[1,1408]{1,0:T(2,128)(2,1)S(1)}, u32[]{:S(2)}, u32[]{:S(2)}) collective-permute-start(bf16[1,1408]{1,0:T(2,128)(2,1)S(1)} %get-tuple-element.13), channel_id=1, source_target_pairs={{4,0},{8,4},{12,8},{5,1},{9,5},{13,9},{6,2},{10,6},{14,10},{7,3},{... | collective-permute-start | bytes 8456 | tf_op jit(solution)/shard_map/ppermute | solution.py:33
  158.0 43.0 %copy-start.2 = (bf16[1408,512]{1,0:T(8,128)(2,1)S(1)}, bf16[1408,512]{1,0:T(8,128)(2,1)}, u32[]{:S(2)}) copy-start(bf16[1408,512]{1,0:T(8,128)(2,1)} %copy-done.1) | copy-start | bytes 4325380
  212.4 8.4 %copy-start.3 = (bf16[256,1408]{1,0:T(8,128)(2,1)S(1)}, bf16[256,1408]{1,0:T(8,128)(2,1)}, u32[]{:S(2)}) copy-start(bf16[256,1408]{1,0:T(8,128)(2,1)} %param.9) | copy-start | bytes 2162692
  227.8 4.0 %collective-permute-start.5 = (bf16[1,1408]{1,0:T(2,128)(2,1)S(1)}, bf16[1,1408]{1,0:T(2,128)(2,1)S(1)}, u32[]{:S(2)}, u32[]{:S(2)}) collective-permute-start(bf16[1,1408]{1,0:T(2,128)(2,1)S(1)} %get-tuple-element.10), channel_id=1, source_target_pairs={{0,4},{4,8},{8,12},{1,5},{5,9},{9,13},{2,6},{6,10},{10,14},{3,7},{... | collective-permute-start | bytes 8456 | tf_op jit(solution)/shard_map/ppermute | solution.py:32
  230.4 7.6 %collective-permute-start.6 = (bf16[1,1408]{1,0:T(2,128)(2,1)S(1)}, bf16[1,1408]{1,0:T(2,128)(2,1)S(1)}, u32[]{:S(2)}, u32[]{:S(2)}) collective-permute-start(bf16[1,1408]{1,0:T(2,128)(2,1)S(1)} %get-tuple-element.11), channel_id=1, source_target_pairs={{4,0},{8,4},{12,8},{5,1},{9,5},{13,9},{6,2},{10,6},{14,10},{7,3},{... | collective-permute-start | bytes 8456 | tf_op jit(solution)/shard_map/ppermute | solution.py:33
Sparse Core Ops, SparseCore 0:
  9.5 19.4 all-gather.3
  30.6 170.7 all-gather.5
  202.9 104.9 all-gather.7
  315.0 23.0 reduce-scatter.1
